TPU v7x, 32 devices: a whole 2x2x4 slice. The times are simulated.
32 devices in a mesh: grp: 2 (over y), sp: 4 (over z), tp: 4 (over x, core).
Axes of the slice: x: 2, y: 2, z: 4, core: 2. Of those that a mesh axis runs over, the one named last changes fastest.
Arguments:
- query_first: bfloat16 [1536, 512], P(('grp', 'sp'), 'tp'), parts along dimension 0, may hold values from -172 to 172
- key_first: bfloat16 [1536, 512], P(('grp', 'sp'), 'tp'), parts along dimension 0, may hold values from -7.8 to 7.8
- query_second: bfloat16 [1536, 1024], P(('grp', 'sp'), 'tp'), parts along dimension 0, may hold values from -172 to 172
- key_second: bfloat16 [1536, 1024], P(('grp', 'sp'), 'tp'), parts along dimension 0, may hold values from -7.8 to 7.8
- values: bfloat16 [1536, 2, 512], P(('grp', 'sp'), None, 'tp'), parts along dimension 0, may hold values from -6 to 6
- lambdas: float32 [2, 4], P(None, 'tp'), may hold values from 0.3 to 0.8
- residual: bfloat16 [1536, 2048], P(('grp', 'sp'), 'tp'), parts along dimension 0, may hold values from -130 to 130
- norm_gain: bfloat16 [2048], P('tp'), may hold values from 0.099609375 to 1.8984375
- out_weight: bfloat16 [2, 512, 2048], P(None, 'tp'), may hold values from -0.1875 to 0.1875
- gate_weight: bfloat16 [2048, 5632], P('sp', 'tp'), may hold values from -0.125 to 0.125
- up_weight: bfloat16 [2048, 5632], P('sp', 'tp'), may hold values from -0.125 to 0.125
- down_weight: bfloat16 [5632, 2048], P('tp', 'sp'), may hold values from -0.078125 to 0.078125
Outputs:
- layer_out: bfloat16 [1536, 2048], P(('grp', 'sp'), 'tp'), parts along dimension 0
There are 2 independent parts, one for each index of `grp`. A program takes and returns all parts, laid end to end along the dimension named above; an argument that names none is the same for every part. Nothing has to cross between parts.
All inputs are finite; a program needn't handle non-finite values.
Results may differ from a plain program's by a relative error of at most 0.0065.
Values may be sent and summed in bfloat16 or wider, within the bound.
A program may use at most 128 MiB of HBM per device.

v0:
```python
import jax
import jax.numpy as jnp
from jax import lax
from jax.sharding import PartitionSpec as P

D = 2048


def per_device(
    query_first,
    key_first,
    query_second,
    key_second,
    values,
    lambdas,
    residual,
    norm_gain,
    out_weight,
    gate_weight,
    up_weight,
    down_weight,
):
    tok_rows = query_first.shape[0]
    heads_here = lambdas.shape[1]
    width_first = query_first.shape[1] // (2 * heads_here)
    width_second = query_second.shape[1] // (2 * heads_here)
    value_size = values.shape[2] // heads_here
    offset = lax.axis_index("sp") * tok_rows
    query_pos = offset + lax.broadcasted_iota(jnp.int32, (tok_rows, 1), 0)
    query_groups = (
        query_first.reshape(tok_rows, heads_here, 2, width_first),
        query_second.reshape(tok_rows, heads_here, 2, width_second),
    )
    key_widths = (width_first, width_second)
    start_state = (
        jnp.full((heads_here, 2, tok_rows, 1), -1e30, jnp.float32),
        jnp.zeros((heads_here, 2, tok_rows, 1), jnp.float32),
        jnp.zeros((heads_here, 2, tok_rows, value_size), jnp.float32),
    )
    states = (start_state, start_state)
    pieces = (
        lax.all_gather(key_first, "sp", axis=0, tiled=True),
        lax.all_gather(key_second, "sp", axis=0, tiled=True),
        lax.all_gather(values, "sp", axis=0, tiled=True),
    )
    piece_rows = pieces[0].shape[0]
    key_pos = lax.broadcasted_iota(jnp.int32, (1, piece_rows), 1)
    allowed = key_pos <= query_pos
    value_rows = pieces[2].reshape(piece_rows, 2, heads_here, value_size)
    results = []
    for group_idx in range(2):
        key_width = key_widths[group_idx]
        key_part = pieces[group_idx].reshape(piece_rows, heads_here, 2, key_width)
        scores = jnp.einsum(
            "qhmd,khmd->hmqk", query_groups[group_idx], key_part, preferred_element_type=jnp.float32
        ) * key_width ** (-0.5)
        scores = jnp.where(allowed, scores, -1e30)
        running, totals, weighted = states[group_idx]
        new_peak = jnp.maximum(running, jnp.max(scores, axis=-1, keepdims=True))
        weights = jnp.where(allowed, jnp.exp(scores - new_peak), 0.0)
        totals = jnp.sum(weights, axis=-1, keepdims=True)
        weighted = jnp.einsum(
            "hmqk,khe->hmqe",
            weights.astype(jnp.bfloat16),
            value_rows[:, group_idx],
            preferred_element_type=jnp.float32,
        )
        results.append((new_peak, totals, weighted))
    states = (results[0], results[1])
    map_out = jnp.stack([states[0][2] / states[0][1], states[1][2] / states[1][1]])
    differ = map_out[:, :, 0] - lambdas[:, :, None, None] * map_out[:, :, 1]
    head_scale = lax.rsqrt(jnp.mean(differ * differ, axis=-1, keepdims=True) + 1e-06)
    attended = (0.8 * differ * head_scale).astype(jnp.bfloat16)
    projection = out_weight.reshape(2, heads_here, value_size, out_weight.shape[2])
    mixed_part = jnp.einsum(
        "ghqe,gher->qr", attended, projection, preferred_element_type=jnp.float32
    )
    mixed = lax.psum_scatter(
        mixed_part.astype(jnp.bfloat16), "tp", scatter_dimension=1, tiled=True
    ).astype(jnp.float32)
    stream = residual.astype(jnp.float32) + mixed
    squares = lax.psum(jnp.sum(stream * stream, axis=1), "tp")
    row_scale = lax.rsqrt(squares[:, None] / D + 1e-06)
    normed = (stream * row_scale * norm_gain.astype(jnp.float32)).astype(jnp.bfloat16)
    full_rows = lax.all_gather(normed, "tp", axis=1, tiled=True)
    pieces = (
        lax.all_gather(gate_weight, "sp", axis=0, tiled=True),
        lax.all_gather(up_weight, "sp", axis=0, tiled=True),
    )
    gate = jnp.dot(full_rows, pieces[0], preferred_element_type=jnp.float32)
    up_part = jnp.dot(full_rows, pieces[1], preferred_element_type=jnp.float32)
    hidden = (jax.nn.silu(gate) * up_part).astype(jnp.bfloat16)
    partial_out = jnp.dot(
        hidden,
        lax.all_gather(down_weight, "sp", axis=1, tiled=True),
        preferred_element_type=jnp.float32,
    )
    ffn = lax.psum_scatter(
        partial_out.astype(jnp.bfloat16), "tp", scatter_dimension=1, tiled=True
    ).astype(jnp.float32)
    return (stream + 0.5 * ffn).astype(jnp.bfloat16)


def solution(mesh):
    return jax.shard_map(
        per_device,
        mesh=mesh,
        in_specs=(
            P(("grp", "sp"), "tp"),
            P(("grp", "sp"), "tp"),
            P(("grp", "sp"), "tp"),
            P(("grp", "sp"), "tp"),
            P(("grp", "sp"), None, "tp"),
            P(None, "tp"),
            P(("grp", "sp"), "tp"),
            P("tp"),
            P(None, "tp", None),
            P("sp", "tp"),
            P("sp", "tp"),
            P("tp", "sp"),
        ),
        out_specs=P(("grp", "sp"), "tp"),
        check_vma=False,
    )
```

profile of v0, /device:TPU:0, one launch (start us, length us, event | category | flops | bytes accessed | tf_op | source)
XLA Modules:
  0.0 419.4 jit_solution(9682786560967322755)
XLA Ops:
  7.4 0.1 iota_compare_fusion
  7.6 16.6 %all_gather.23 = bf16[768,256]{1,0:T(8,128)(2,1)S(1)} all-gather(bf16[192,256]{1,0:T(8,128)(2,1)} %param.15), channel_id=1, replica_groups=mesh['grp'=2,'sp'=4,'tp'=4] {'sp'}, dimensions={0}, use_global_device_ids=true | all-gather | bytes 491520 | tf_op jit(solution)/shard_map/all_gather | solution.py:43
  24.2 0.2 copy.28
  24.4 14.4 %all_gather.21 = bf16[768,128]{1,0:T(8,128)(2,1)S(1)} all-gather(bf16[192,128]{1,0:T(8,128)(2,1)S(1)} %copy-done.6), channel_id=1, replica_groups=mesh['grp'=2,'sp'=4,'tp'=4] {'sp'}, dimensions={0}, use_global_device_ids=true | all-gather | bytes 245760 | tf_op jit(solution)/shard_map/all_gather | solution.py:42
  38.8 0.1 copy.26
  38.9 0.1 copy.25
  39.1 14.8 %all_gather.22 = bf16[768,2,128]{2,0,1:T(8,128)(2,1)S(1)} all-gather(bf16[192,2,128]{2,0,1:T(8,128)(2,1)S(1)} %copy.27), channel_id=1, replica_groups=mesh['grp'=2,'sp'=4,'tp'=4] {'sp'}, dimensions={0}, use_global_device_ids=true | all-gather | bytes 491520 | tf_op jit(solution)/shard_map/all_gather | solution.py:44
  53.8 0.5 fusion.34
  54.3 0.5 fusion.35
  54.8 0.7 fusion.6
  55.5 0.4 fusion.5
  55.9 0.4 fusion.4
  56.4 0.2 copy-done.7
  56.6 0.2 fusion.21
  56.8 1.3 fusion
  58.2 0.0 all-gather.4.cloned.1.call-start
  58.3 0.5 all-gather.4.cloned.1.call-update
  58.9 0.5 all-gather.6.cloned.1.call-update
  59.4 0.5 all-gather.8.cloned.1.call-update
  60.0 0.0 reduce-scatter.5.cloned.1.call-start
  60.0 22.8 %reduce-scatter.3.cloned.1.call-done = bf16[192,512]{1,0:T(8,128)(2,1)} async-done(((bf16[192,2048]{1,0:T(8,128)(2,1)}), bf16[192,512]{1,0:T(8,128)(2,1)}) %reduce-scatter.3.cloned.1.call-update) | async-done | bytes 196624 | tf_op jit(solution)/shard_map/reduce_scatter | solution.py:78
  82.8 1.1 multiply_reduce_fusion
  83.9 6.1 %psum.7 = f32[192]{0:T(256)S(1)} all-reduce(f32[192]{0:T(256)S(1)} %multiply_reduce_fusion), channel_id=1, replica_groups=mesh['grp'=2,'sp'=4,'tp'=4] {'tp'}, use_global_device_ids=true, to_apply=%region_7.8 | all-reduce | flops 192 | bytes 1536 | tf_op jit(solution)/shard_map/psum | solution.py:82
  90.0 1.0 multiply_convert_fusion
  91.0 8.4 %all_gather.24 = bf16[192,2048]{1,0:T(8,128)(2,1)S(1)} all-gather(bf16[192,512]{1,0:T(8,128)(2,1)S(1)} %multiply_convert_fusion), channel_id=1, replica_groups=mesh['grp'=2,'sp'=4,'tp'=4] {'tp'}, dimensions={1}, use_global_device_ids=true | all-gather | bytes 983040 | tf_op jit(solution)/shard_map/all_gather | solution.py:85
  99.4 68.7 %all-gather.4.cloned.1.call-done = bf16[2048,1408]{1,0:T(8,128)(2,1)} async-done(((bf16[512,1408]{1,0:T(8,128)(2,1)}), bf16[2048,1408]{1,0:T(8,128)(2,1)}) %all-gather.4.cloned.1.call-update) | async-done | bytes 5767184 | tf_op jit(solution)/shard_map/all_gather | solution.py:87
  168.1 4.0 fusion.36
  172.1 102.2 %all-gather.6.cloned.1.call-done = bf16[2048,1408]{1,0:T(8,128)(2,1)} async-done(((bf16[512,1408]{1,0:T(8,128)(2,1)}), bf16[2048,1408]{1,0:T(8,128)(2,1)}) %all-gather.6.cloned.1.call-update) | async-done | bytes 5767184 | tf_op jit(solution)/shard_map/all_gather | solution.py:88
  274.4 106.3 %all-gather.8.cloned.1.call-done = bf16[1408,2048]{1,0:T(8,128)(2,1)} async-done(((bf16[1408,512]{1,0:T(8,128)(2,1)}), bf16[1408,2048]{1,0:T(8,128)(2,1)}) %all-gather.8.cloned.1.call-update) | async-done | bytes 5767184 | tf_op jit(solution)/shard_map/all_gather | solution.py:95
  380.6 7.9 %convolution_convert_fusion = bf16[192,2048]{1,0:T(8,128)(2,1)} fusion(bf16[1408,2048]{1,0:T(8,128)(2,1)} %all-gather.8.cloned.1.call-done, bf16[192,2048]{1,0:T(8,128)(2,1)S(1)} %all_gather.24, bf16[2048,1408]{1,0:T(8,128)(2,1)} %all-gather.6.cloned.1.call-done, f32[192,1408]{1,0:T(8,128)S(1)} %fusion.36), kind=kOutput, calls=%fused_computation.4 | convolution fusion | flops 2216607744 | bytes 14188544 | tf_op jit(solution)/shard_map/dot_general | solution.py:93
  388.5 21.6 %reduce-scatter.5.cloned.1.call-done = bf16[192,512]{1,0:T(8,128)(2,1)} async-done(((bf16[192,2048]{1,0:T(8,128)(2,1)}), bf16[192,512]{1,0:T(8,128)(2,1)}) %reduce-scatter.5.cloned.1.call-update) | async-done | bytes 196624 | tf_op jit(solution)/shard_map/reduce_scatter | solution.py:98
  410.2 1.7 add_convert_fusion
  (28 shorter events, 0.2 us)
Async XLA Ops:
  7.4 49.5 %copy-start = (bf16[2,128,2048]{2,1,0:T(8,128)(2,1)S(1)}, bf16[2,128,2048]{2,1,0:T(8,128)(2,1)}, u32[]{:S(2)}) copy-start(bf16[2,128,2048]{2,1,0:T(8,128)(2,1)} %param.20) | copy-start | bytes 3145732
  7.4 17.0 %copy-start.6 = (bf16[192,128]{1,0:T(8,128)(2,1)S(1)}, bf16[192,128]{1,0:T(8,128)(2,1)}, u32[]{:S(2)}) copy-start(bf16[192,128]{1,0:T(8,128)(2,1)} %param.13) | copy-start | bytes 147460
  7.4 31.5 %copy-start.5 = (bf16[192,128]{1,0:T(8,128)(2,1)S(1)}, bf16[192,128]{1,0:T(8,128)(2,1)}, u32[]{:S(2)}) copy-start(bf16[192,128]{1,0:T(8,128)(2,1)} %param.12) | copy-start | bytes 147460
  7.4 31.7 %copy-start.4 = (bf16[192,2,128]{2,1,0:T(2,128)(2,1)S(1)}, bf16[192,2,128]{2,1,0:T(2,128)(2,1)}, u32[]{:S(2)}) copy-start(bf16[192,2,128]{2,1,0:T(2,128)(2,1)} %param.16) | copy-start | bytes 294916
  7.4 75.4 %reduce-scatter.3.cloned.1.call-start = ((), (), s32[]{:S(2)}) async-start(), calls=%async_computation.2 | async-start | bytes 983040 | tf_op jit(solution)/shard_map/reduce_scatter | solution.py:78
  24.2 29.6 %copy-start.3 = (bf16[192,256]{1,0:T(8,128)(2,1)S(1)}, bf16[192,256]{1,0:T(8,128)(2,1)}, u32[]{:S(2)}) copy-start(bf16[192,256]{1,0:T(8,128)(2,1)} %param.14) | copy-start | bytes 294916
  55.9 0.7 copy-start.7
  58.2 109.9 %all-gather.4.cloned.1.call-start = ((), (), s32[]{:S(2)}) async-start(), calls=%async_computation.3 | async-start | bytes 7208960 | tf_op jit(solution)/shard_map/all_gather | solution.py:87
  58.8 1.2 copy-start.8
  58.8 24.0 %copy-start.1 = (bf16[192,512]{1,0:T(8,128)(2,1)S(1)}, bf16[192,512]{1,0:T(8,128)(2,1)}, u32[]{:S(2)}) copy-start(bf16[192,512]{1,0:T(8,128)(2,1)} %param.18) | copy-start | bytes 589828
  58.8 215.6 %all-gather.6.cloned.1.call-start = ((), (), s32[]{:S(2)}) async-start(), calls=%async_computation.4 | async-start | bytes 7208960 | tf_op jit(solution)/shard_map/all_gather | solution.py:88
  59.4 321.3 %all-gather.8.cloned.1.call-start = ((), (), s32[]{:S(2)}) async-start(), calls=%async_computation.5 | async-start | bytes 7208960 | tf_op jit(solution)/shard_map/all_gather | solution.py:95
  60.0 350.2 %reduce-scatter.5.cloned.1.call-start = ((), (), s32[]{:S(2)}) async-start(), calls=%async_computation.6 | async-start | bytes 983040 | tf_op jit(solution)/shard_map/reduce_scatter | solution.py:98
  172.1 238.0 %copy-start.2 = (bf16[192,512]{1,0:T(8,128)(2,1)S(1)}, bf16[192,512]{1,0:T(8,128)(2,1)}, u32[]{:S(2)}) copy-start(bf16[192,512]{1,0:T(8,128)(2,1)} %reduce-scatter.3.cloned.1.call-done) | copy-start | bytes 589828
Sparse Core Ops, SparseCore 0:
  58.3 24.4 reduce-scatter.2
  388.7 21.4 reduce-scatter.4
Sparse Core Ops, SparseCore 1:
  60.3 107.8 all-gather.3
  169.5 104.8 all-gather.5
  275.8 104.8 all-gather.7
where the time goes:
time: 420 us; the launch traced here: 419 us
  waiting for transfers between devices  323 us (77%)
  blocking collectives  60.2 us (14%)
  between operations  15.2 us (4%)
  matrix products  15.1 us (4%)
  other arithmetic  4.87 us (1%)
    all_gather x1, waiting for transfers between devices, per_device(): lax.all_gather(down_weight, 'sp', axis=1, tiled=True)  106 us
    all_gather x1, waiting for transfers between devices, per_device(): lax.all_gather(up_weight, 'sp', axis=0, tiled=True)  102 us
    all_gather x1, waiting for transfers between devices, per_device(): lax.all_gather(gate_weight, 'sp', axis=0, tiled=True)  68.7 us
    reduce_scatter x1, waiting for transfers between devices, per_device(): lax.psum_scatter(mixed_part.astype(jnp.bfloat16), 'tp', scatter_dimension...  22.8 us
    reduce_scatter x1, waiting for transfers between devices, per_device(): lax.psum_scatter(partial_out.astype(jnp.bfloat16), 'tp', scatter_dimensio...  21.6 us
    all_gather x1, blocking collectives, per_device(): lax.all_gather(key_second, 'sp', axis=0, tiled=True)  16.6 us
    all_gather x1, blocking collectives, per_device(): lax.all_gather(values, 'sp', axis=0, tiled=True)  14.8 us
    all_gather x1, blocking collectives, per_device(): lax.all_gather(key_first, 'sp', axis=0, tiled=True)  14.4 us
  transfers between devices with their start and end apart: 5, of which 5 were waited for; matrix products, arithmetic and copies ran while one was open for 1% of the time, Pallas kernels for 0%

commit v1 on v0

--- a/solution.py
+++ b/solution.py
@@ -4,6 +4,27 @@
 from jax.sharding import PartitionSpec as P
 
 D = 2048
+
+
+def gather_around(x, axis, dim):
+    size, here, width = (lax.axis_size(axis), lax.axis_index(axis), x.shape[dim])
+    right = [(i, (i + 1) % size) for i in range(size)]
+    downward = [(i, (i - 1) % size) for i in range(size)]
+    filled = jnp.zeros((*x.shape[:dim], size * width, *x.shape[dim + 1 :]), x.dtype)
+    filled = lax.dynamic_update_slice_in_dim(filled, x, here * width, axis=dim)
+    from_left = from_right = x
+    middle = size // 2
+    for step in range(1, middle + 1):
+        from_left = lax.ppermute(from_left, axis, right)
+        filled = lax.dynamic_update_slice_in_dim(
+            filled, from_left, (here - step) % size * width, axis=dim
+        )
+        if step < size - middle:
+            from_right = lax.ppermute(from_right, axis, downward)
+            filled = lax.dynamic_update_slice_in_dim(
+                filled, from_right, (here + step) % size * width, axis=dim
+            )
+    return filled
 
 
 def per_device(
@@ -91,9 +112,7 @@
     up_part = jnp.dot(full_rows, pieces[1], preferred_element_type=jnp.float32)
     hidden = (jax.nn.silu(gate) * up_part).astype(jnp.bfloat16)
     partial_out = jnp.dot(
-        hidden,
-        lax.all_gather(down_weight, "sp", axis=1, tiled=True),
-        preferred_element_type=jnp.float32,
+        hidden, gather_around(down_weight, "sp", 1), preferred_element_type=jnp.float32
     )
     ffn = lax.psum_scatter(
         partial_out.astype(jnp.bfloat16), "tp", scatter_dimension=1, tiled=True

time: 420 us -> 387 us (0.921)
  waiting for transfers between devices: 323 us -> 227 us
  starting transfers between devices: 0.2 us -> 49.7 us
  local copies, waits for them, and re-layouts: 0.68 us -> 13.1 us
    all_gather x1 -> x0, waiting for transfers between devices: 106 us -> none  [per_device(): lax.all_gather(down_weight, 'sp', axis=1, tiled=True)]
    ppermute x0 -> x3, waiting for transfers between devices: none -> 95.6 us  [the longest x2 65.5 us: gather_around(): from_left = lax.ppermute(from_left, axis, right)]
    all_gather x1, waiting for transfers between devices: 68.7 us -> 7.25 us  [per_device(): lax.all_gather(gate_weight, 'sp', axis=0, tiled=True)]
    ppermute x0 -> x3, starting transfers between devices: none -> 49.6 us  [the longest x2 47.5 us: gather_around(): from_left = lax.ppermute(from_left, axis, right)]
    reduce_scatter x1, waiting for transfers between devices: 22.8 us -> 0.01 us  [per_device(): lax.psum_scatter(mixed_part.astype(jnp.bfloat16), 'tp', scatter_dimension...]
    dynamic_update_slice x0 -> x4, local copies, waits for them, and re-layouts: none -> 9.13 us  [the longest x2 5.28 us: gather_around(): lax.dynamic_update_slice_in_dim(filled, from_left, (here - step) % size *...]
  transfers between devices with their start and end apart: 5 -> 7, of which waited for: 5 -> 6; matrix products, arithmetic and copies ran while one was open for 1% -> 5% of each run, Pallas kernels for 0% -> 0%
where the time goes in v1:
time: 387 us
  waiting for transfers between devices  227 us (59%)
  blocking collectives  60.4 us (16%)
  starting transfers between devices  49.7 us (13%)
  matrix products  16.4 us (4%)
  between operations  15 us (4%)
  local copies, waits for them, and re-layouts  13.1 us (3%)
  other arithmetic  4.87 us (1%)
    all_gather x1, waiting for transfers between devices, per_device(): lax.all_gather(up_weight, 'sp', axis=0, tiled=True)  102 us
    ppermute x2, waiting for transfers between devices, gather_around(): from_left = lax.ppermute(from_left, axis, right)  65.5 us
    ppermute x2, starting transfers between devices, gather_around(): from_left = lax.ppermute(from_left, axis, right)  47.5 us
    ppermute x1, waiting for transfers between devices, gather_around(): from_right = lax.ppermute(from_right, axis, downward)  30.1 us
    reduce_scatter x1, waiting for transfers between devices, per_device(): lax.psum_scatter(partial_out.astype(jnp.bfloat16), 'tp', scatter_dimensio...  21.6 us
    all_gather x1, blocking collectives, per_device(): lax.all_gather(key_second, 'sp', axis=0, tiled=True)  16.6 us
    all_gather x1, blocking collectives, per_device(): lax.all_gather(values, 'sp', axis=0, tiled=True)  14.8 us
    all_gather x1, blocking collectives, per_device(): lax.all_gather(key_first, 'sp', axis=0, tiled=True)  14.4 us
  transfers between devices with their start and end apart: 7, of which 6 were waited for; matrix products, arithmetic and copies ran while one was open for 5% of the time, Pallas kernels for 0%

profile of v1, /device:TPU:0, one launch (start us, length us, event | category | flops | bytes accessed | tf_op | source)
XLA Modules:
  0.0 386.8 jit_solution(16229555358143967344)
XLA Ops:
  7.6 16.6 %all_gather.20 = bf16[768,256]{1,0:T(8,128)(2,1)S(1)} all-gather(bf16[192,256]{1,0:T(8,128)(2,1)} %param.15), channel_id=1, replica_groups=mesh['grp'=2,'sp'=4,'tp'=4] {'sp'}, dimensions={0}, use_global_device_ids=true | all-gather | bytes 491520 | tf_op jit(solution)/shard_map/all_gather | solution.py:64
  24.4 14.4 %all_gather.18 = bf16[768,128]{1,0:T(8,128)(2,1)S(1)} all-gather(bf16[192,128]{1,0:T(8,128)(2,1)S(1)} %copy-done.7), channel_id=1, replica_groups=mesh['grp'=2,'sp'=4,'tp'=4] {'sp'}, dimensions={0}, use_global_device_ids=true | all-gather | bytes 245760 | tf_op jit(solution)/shard_map/all_gather | solution.py:63
  39.1 14.8 %all_gather.19 = bf16[768,2,128]{2,0,1:T(8,128)(2,1)S(1)} all-gather(bf16[192,2,128]{2,0,1:T(8,128)(2,1)S(1)} %copy.27), channel_id=1, replica_groups=mesh['grp'=2,'sp'=4,'tp'=4] {'sp'}, dimensions={0}, use_global_device_ids=true | all-gather | bytes 491520 | tf_op jit(solution)/shard_map/all_gather | solution.py:65
  53.8 0.5 fusion.34
  54.3 0.5 fusion.35
  54.8 0.7 fusion.6
  55.5 0.4 fusion.4
  55.9 0.4 fusion.5
  56.8 1.3 fusion
  58.3 0.5 all-gather.3.cloned.1.call-update
  58.9 0.5 all-gather.5.cloned.1.call-update
  59.6 2.0 collective-permute-start
  61.5 2.1 collective-permute-start.1
  63.6 3.2 broadcast_in_dim.34
  66.8 1.2 constant_dynamic-update-slice_fusion.3
  68.0 49.0 %collective-permute-done = bf16[1408,512]{1,0:T(8,128)(2,1)} collective-permute-done((bf16[1408,512]{1,0:T(8,128)(2,1)S(1)}, bf16[1408,512]{1,0:T(8,128)(2,1)}, u32[]{:S(2)}, u32[]{:S(2)}) %collective-permute-start) | collective-permute-done | bytes 1441824 | tf_op jit(solution)/shard_map/ppermute | solution.py:18
  117.0 45.5 %collective-permute-start.2 = (bf16[1408,512]{1,0:T(8,128)(2,1)}, bf16[1408,512]{1,0:T(8,128)(2,1)}, u32[]{:S(2)}, u32[]{:S(2)}) collective-permute-start(bf16[1408,512]{1,0:T(8,128)(2,1)} %collective-permute-done), channel_id=1, source_target_pairs={{0,4},{4,8},{8,12},{12,0},{1,5},{5,9},{9,13},{13,1},{2,6},{6,10},{... | collective-permute-start | bytes 4325384 | tf_op jit(solution)/shard_map/ppermute | solution.py:18
  162.5 2.7 constant_dynamic-update-slice_fusion.2
  165.2 30.1 %collective-permute-done.1 = bf16[1408,512]{1,0:T(8,128)(2,1)} collective-permute-done((bf16[1408,512]{1,0:T(8,128)(2,1)S(1)}, bf16[1408,512]{1,0:T(8,128)(2,1)}, u32[]{:S(2)}, u32[]{:S(2)}) %collective-permute-start.1) | collective-permute-done | bytes 1441824 | tf_op jit(solution)/shard_map/ppermute | solution.py:23
  195.3 2.6 constant_dynamic-update-slice_fusion.1
  197.9 1.1 multiply_reduce_fusion
  199.0 6.1 %psum.7 = f32[192]{0:T(256)S(1)} all-reduce(f32[192]{0:T(256)S(1)} %multiply_reduce_fusion), channel_id=1, replica_groups=mesh['grp'=2,'sp'=4,'tp'=4] {'tp'}, use_global_device_ids=true, to_apply=%region_7.8 | all-reduce | flops 192 | bytes 1536 | tf_op jit(solution)/shard_map/psum | solution.py:103
  205.1 1.0 multiply_convert_fusion
  206.1 8.6 %all_gather.21 = bf16[192,2048]{1,0:T(8,128)(2,1)S(1)} all-gather(bf16[192,512]{1,0:T(8,128)(2,1)S(1)} %multiply_convert_fusion), channel_id=1, replica_groups=mesh['grp'=2,'sp'=4,'tp'=4] {'tp'}, dimensions={1}, use_global_device_ids=true | all-gather | bytes 983040 | tf_op jit(solution)/shard_map/all_gather | solution.py:106
  214.7 16.5 %collective-permute-done.2 = bf16[1408,512]{1,0:T(8,128)(2,1)} collective-permute-done((bf16[1408,512]{1,0:T(8,128)(2,1)}, bf16[1408,512]{1,0:T(8,128)(2,1)}, u32[]{:S(2)}, u32[]{:S(2)}) %collective-permute-start.2) | collective-permute-done | bytes 1441824 | tf_op jit(solution)/shard_map/ppermute | solution.py:18
  231.2 2.6 constant_dynamic-update-slice_fusion
  233.8 7.2 %all-gather.3.cloned.1.call-done = bf16[2048,1408]{1,0:T(8,128)(2,1)} async-done(((bf16[512,1408]{1,0:T(8,128)(2,1)}), bf16[2048,1408]{1,0:T(8,128)(2,1)}) %all-gather.3.cloned.1.call-update) | async-done | bytes 5767184 | tf_op jit(solution)/shard_map/all_gather | solution.py:108
  241.1 5.0 %fusion.36 = f32[192,1408]{1,0:T(8,128)} fusion(bf16[192,2048]{1,0:T(8,128)(2,1)S(1)} %all_gather.21, bf16[2048,1408]{1,0:T(8,128)(2,1)} %all-gather.3.cloned.1.call-done), kind=kOutput, calls=%fused_computation.64 | convolution fusion | flops 1107296256 | bytes 7634944 | tf_op jit(solution)/shard_map/dot_general | solution.py:111
  246.1 101.7 %all-gather.5.cloned.1.call-done = bf16[2048,1408]{1,0:T(8,128)(2,1)} async-done(((bf16[512,1408]{1,0:T(8,128)(2,1)}), bf16[2048,1408]{1,0:T(8,128)(2,1)}) %all-gather.5.cloned.1.call-update) | async-done | bytes 5767184 | tf_op jit(solution)/shard_map/all_gather | solution.py:109
  347.8 8.2 %convolution_convert_fusion = bf16[192,2048]{1,0:T(8,128)(2,1)} fusion(bf16[1408,2048]{1,0:T(8,128)(2,1)} %constant_dynamic-update-slice_fusion, bf16[192,2048]{1,0:T(8,128)(2,1)S(1)} %all_gather.21, bf16[2048,1408]{1,0:T(8,128)(2,1)} %all-gather.5.cloned.1.call-done, f32[192,1408]{1,0:T(8,128)} %fusion.36), kind=kOutput, calls=%fused_computation.4 | convolution fusion | flops 2216607744 | bytes 14188544 | tf_op jit(solution)/shard_map/dot_general | solution.py:114
  356.0 21.6 %reduce-scatter.5.cloned.1.call-done = bf16[192,512]{1,0:T(8,128)(2,1)} async-done(((bf16[192,2048]{1,0:T(8,128)(2,1)}), bf16[192,512]{1,0:T(8,128)(2,1)}) %reduce-scatter.5.cloned.1.call-update) | async-done | bytes 196624 | tf_op jit(solution)/shard_map/reduce_scatter | solution.py:117
  377.6 1.7 add_convert_fusion
  (38 shorter events, 1.4 us)
Async XLA Ops:
  7.4 49.5 %copy-start = (bf16[2,128,2048]{2,1,0:T(8,128)(2,1)S(1)}, bf16[2,128,2048]{2,1,0:T(8,128)(2,1)}, u32[]{:S(2)}) copy-start(bf16[2,128,2048]{2,1,0:T(8,128)(2,1)} %param.20) | copy-start | bytes 3145732
  7.4 17.0 %copy-start.7 = (bf16[192,128]{1,0:T(8,128)(2,1)S(1)}, bf16[192,128]{1,0:T(8,128)(2,1)}, u32[]{:S(2)}) copy-start(bf16[192,128]{1,0:T(8,128)(2,1)} %param.13) | copy-start | bytes 147460
  7.4 31.5 %copy-start.6 = (bf16[192,128]{1,0:T(8,128)(2,1)S(1)}, bf16[192,128]{1,0:T(8,128)(2,1)}, u32[]{:S(2)}) copy-start(bf16[192,128]{1,0:T(8,128)(2,1)} %param.12) | copy-start | bytes 147460
  7.4 31.7 %copy-start.5 = (bf16[192,2,128]{2,1,0:T(2,128)(2,1)S(1)}, bf16[192,2,128]{2,1,0:T(2,128)(2,1)}, u32[]{:S(2)}) copy-start(bf16[192,2,128]{2,1,0:T(2,128)(2,1)} %param.16) | copy-start | bytes 294916
  7.4 190.5 %reduce-scatter.3.cloned.1.call-start = ((), (), s32[]{:S(2)}) async-start(), calls=%async_computation.2 | async-start | bytes 983040 | tf_op jit(solution)/shard_map/reduce_scatter | solution.py:99
  24.2 29.6 %copy-start.4 = (bf16[192,256]{1,0:T(8,128)(2,1)S(1)}, bf16[192,256]{1,0:T(8,128)(2,1)}, u32[]{:S(2)}) copy-start(bf16[192,256]{1,0:T(8,128)(2,1)} %param.14) | copy-start | bytes 294916
  55.9 0.7 copy-start.8
  58.2 1.4 copy-start.3
  58.2 5.4 %copy-start.9 = (bf16[512]{0:T(512)(128)(2,1)S(1)}, bf16[512]{0:T(512)(128)(2,1)}, u32[]{:S(2)}) copy-start(bf16[512]{0:T(512)(128)(2,1)} %param.19) | copy-start | bytes 3076
  58.2 182.9 %all-gather.3.cloned.1.call-start = ((), (), s32[]{:S(2)}) async-start(), calls=%async_computation.3 | async-start | bytes 7208960 | tf_op jit(solution)/shard_map/all_gather | solution.py:108
  58.8 289.0 %all-gather.5.cloned.1.call-start = ((), (), s32[]{:S(2)}) async-start(), calls=%async_computation.4 | async-start | bytes 7208960 | tf_op jit(solution)/shard_map/all_gather | solution.py:109
  59.4 318.2 %reduce-scatter.5.cloned.1.call-start = ((), (), s32[]{:S(2)}) async-start(), calls=%async_computation.5 | async-start | bytes 983040 | tf_op jit(solution)/shard_map/reduce_scatter | solution.py:117
  59.6 57.4 %collective-permute-start = (bf16[1408,512]{1,0:T(8,128)(2,1)S(1)}, bf16[1408,512]{1,0:T(8,128)(2,1)}, u32[]{:S(2)}, u32[]{:S(2)}) collective-permute-start(bf16[1408,512]{1,0:T(8,128)(2,1)S(1)} %copy-done.3), channel_id=1, source_target_pairs={{0,4},{4,8},{8,12},{12,0},{1,5},{5,9},{9,13},{13,1},{2,6},{6,10},{... | collective-permute-start | bytes 4325384 | tf_op jit(solution)/shard_map/ppermute | solution.py:18
  61.5 133.8 %collective-permute-start.1 = (bf16[1408,512]{1,0:T(8,128)(2,1)S(1)}, bf16[1408,512]{1,0:T(8,128)(2,1)}, u32[]{:S(2)}, u32[]{:S(2)}) collective-permute-start(bf16[1408,512]{1,0:T(8,128)(2,1)S(1)} %copy-done.3), channel_id=1, source_target_pairs={{0,12},{4,0},{8,4},{12,8},{1,13},{5,1},{9,5},{13,9},{2,14},{6,2},{... | collective-permute-start | bytes 4325384 | tf_op jit(solution)/shard_map/ppermute | solution.py:23
  117.0 114.3 %collective-permute-start.2 = (bf16[1408,512]{1,0:T(8,128)(2,1)}, bf16[1408,512]{1,0:T(8,128)(2,1)}, u32[]{:S(2)}, u32[]{:S(2)}) collective-permute-start(bf16[1408,512]{1,0:T(8,128)(2,1)} %collective-permute-done), channel_id=1, source_target_pairs={{0,4},{4,8},{8,12},{12,0},{1,5},{5,9},{9,13},{13,1},{2,6},{6,10},{... | collective-permute-start | bytes 4325384 | tf_op jit(solution)/shard_map/ppermute | solution.py:18
  165.1 32.8 %copy-start.1 = (bf16[192,512]{1,0:T(8,128)(2,1)S(1)}, bf16[192,512]{1,0:T(8,128)(2,1)}, u32[]{:S(2)}) copy-start(bf16[192,512]{1,0:T(8,128)(2,1)} %param.18) | copy-start | bytes 589828
  246.1 131.5 %copy-start.2 = (bf16[192,512]{1,0:T(8,128)(2,1)S(1)}, bf16[192,512]{1,0:T(8,128)(2,1)}, u32[]{:S(2)}) copy-start(bf16[192,512]{1,0:T(8,128)(2,1)} %reduce-scatter.3.cloned.1.call-done) | copy-start | bytes 589828
Sparse Core Ops, SparseCore 0:
  58.3 24.8 reduce-scatter.2
  356.1 21.4 reduce-scatter.4
Sparse Core Ops, SparseCore 1:
  60.3 180.8 all-gather.2
  242.5 105.2 all-gather.4
